TPU v7x, 32 devices: a whole 2x2x4 slice. The times are simulated.
32 devices in a mesh: grp: 2 (over x), row: 4 (over z), col: 4 (over y, core).
Axes of the slice: x: 2, y: 2, z: 4, core: 2. Of those that a mesh axis runs over, the one named last changes fastest.
Arguments:
- tokens: bfloat16 [2, 2048, 2048], P('grp', ('row', 'col')), parts along dimension 0, may hold values from -6 to 6
- norm_gain: bfloat16 [2048], replicated, may hold values from 0.099609375 to 1.8984375
- w_in: bfloat16 [2048, 512], replicated, may hold values from -0.125 to 0.125
- w_out: bfloat16 [512, 2048], replicated, may hold values from -0.25 to 0.25
Outputs:
- mixed: bfloat16 [2, 2048, 2048], P('grp', ('row', 'col')), parts along dimension 0
There are 2 independent parts, one for each index of `grp`. A program takes and returns all parts, laid end to end along the dimension named above; an argument that names none is the same for every part. Nothing has to cross between parts.
All inputs are finite; a program needn't handle non-finite values.
Results may differ from a plain program's by a relative error of at most 0.013.
Values may be sent and summed in bfloat16 or wider, within the bound.
A program may use at most 64 MiB of HBM per device.

v0:
```python
import math

import jax
import jax.numpy as jnp
from jax import lax
from jax.sharding import PartitionSpec as P

GROUP_CH = 128


TWO_PI = 2.0 * math.pi
NORM_EPS = 1e-06
HIGHEST = lax.Precision.HIGHEST


def phase_tables(rows, cols, period):
    left = lax.broadcasted_iota(jnp.int32, (rows, cols), 0)
    right = lax.broadcasted_iota(jnp.int32, (rows, cols), 1)
    angles = (left * right % period).astype(jnp.float32) * (TWO_PI / period)
    return (jnp.cos(angles), jnp.sin(angles))


def rotate_by(pattern, cos_table, sin_table, real_part, imag_part):

    def apply(table, data):
        return jnp.einsum(pattern, table, data, precision=HIGHEST)

    return (
        apply(cos_table, real_part) + apply(sin_table, imag_part),
        apply(cos_table, imag_part) - apply(sin_table, real_part),
    )


def twist(real_part, imag_part, cos_table, sin_table):
    return (
        real_part * cos_table + imag_part * sin_table,
        imag_part * cos_table - real_part * sin_table,
    )


def shards(tokens, norm_gain, w_in, w_out):
    seq_count, tok_count, width = tokens.shape
    feat_count = w_in.shape[1]
    row_count = lax.axis_size("row")
    col_count = lax.axis_size("col")
    block_len = tok_count * col_count
    length = block_len * row_count
    sub_feats = feat_count // row_count
    fine_count = tok_count // row_count
    item_count = seq_count * feat_count // col_count
    ortho_scale = 1.0 / math.sqrt(length * GROUP_CH)
    widened = tokens.astype(jnp.float32)
    factor = lax.rsqrt(jnp.mean(widened * widened, -1, keepdims=True) + NORM_EPS)
    normed = (widened * factor * norm_gain.astype(jnp.float32)).astype(jnp.bfloat16)
    mixin = jnp.einsum("std,df->sft", normed, w_in, preferred_element_type=jnp.float32).astype(
        jnp.bfloat16
    )
    row_cos, row_sin = phase_tables(row_count, row_count, row_count)
    chan_cos, chan_sin = phase_tables(GROUP_CH, GROUP_CH, GROUP_CH)
    stacked_shape = (seq_count, sub_feats, row_count, tok_count)
    grouped = mixin.astype(jnp.float32).reshape(
        seq_count, feat_count // GROUP_CH, GROUP_CH, tok_count
    )
    spec_real = jnp.einsum("sgqt,qm->sgmt", grouped, chan_cos, precision=HIGHEST).reshape(
        seq_count, feat_count, tok_count
    )
    spec_imag = -jnp.einsum("sgqt,qm->sgmt", grouped, chan_sin, precision=HIGHEST).reshape(
        seq_count, feat_count, tok_count
    )
    arrived = (
        lax.all_to_all(
            spec_real.astype(jnp.bfloat16), "row", split_axis=1, concat_axis=2, tiled=True
        ).astype(spec_real.dtype),
        lax.all_to_all(
            spec_imag.astype(jnp.bfloat16), "row", split_axis=1, concat_axis=2, tiled=True
        ).astype(spec_imag.dtype),
    )
    stacked_real = arrived[0].reshape(stacked_shape)
    stacked_imag = arrived[1].reshape(stacked_shape)
    real_part, imag_part = rotate_by("ka,sfat->skft", row_cos, row_sin, stacked_real, stacked_imag)
    freq_low = lax.broadcasted_iota(jnp.int32, (row_count, tok_count), 0)
    place = lax.axis_index("col") * tok_count + lax.broadcasted_iota(
        jnp.int32, (row_count, tok_count), 1
    )
    angles = (freq_low * place % length).astype(jnp.float32) * (TWO_PI / length)
    real_part, imag_part = twist(
        real_part, imag_part, jnp.cos(angles)[None, :, None, :], jnp.sin(angles)[None, :, None, :]
    )
    sending = (
        real_part.reshape(item_count, col_count, 1, tok_count),
        imag_part.reshape(item_count, col_count, 1, tok_count),
    )
    col_cos, col_sin = phase_tables(col_count, col_count, col_count)
    mid_cos, mid_sin = phase_tables(col_count, tok_count, block_len)
    tok_cos, tok_sin = phase_tables(tok_count, tok_count, tok_count)
    tok_cos = tok_cos.reshape(row_count, fine_count, tok_count)
    tok_sin = tok_sin.reshape(row_count, fine_count, tok_count)
    span_real, span_imag = rotate_by(
        "uc,qct->qut",
        col_cos,
        col_sin,
        lax.all_to_all(
            sending[0].astype(jnp.bfloat16), "col", split_axis=1, concat_axis=2, tiled=True
        ).astype(jnp.float32)[:, 0],
        lax.all_to_all(
            sending[1].astype(jnp.bfloat16), "col", split_axis=1, concat_axis=2, tiled=True
        ).astype(jnp.float32)[:, 0],
    )
    span_real, span_imag = twist(span_real, span_imag, mid_cos, mid_sin)
    span_real, span_imag = rotate_by("rjt,qut->rjuq", tok_cos, tok_sin, span_real, span_imag)
    owner_shape = (row_count, col_count, fine_count, span_real.shape[-1], 1)
    span_real, span_imag = (span_real.reshape(owner_shape), span_imag.reshape(owner_shape))
    rounded = (span_real * ortho_scale).astype(jnp.bfloat16)
    returned = lax.all_to_all(rounded, "col", split_axis=1, concat_axis=4, tiled=True)
    layout = (row_count, fine_count, seq_count, row_count, sub_feats)
    spectrum = lax.all_to_all(
        returned.reshape(layout), "row", split_axis=0, concat_axis=4, tiled=True
    )
    spectrum = spectrum.reshape(fine_count, seq_count, row_count, feat_count)
    mixed = jnp.einsum("jskf,fd->sjkd", spectrum, w_out, preferred_element_type=jnp.float32).astype(
        jnp.bfloat16
    )
    return mixed.reshape(seq_count, fine_count * row_count, width)


def solution(mesh):
    return jax.shard_map(
        shards,
        mesh=mesh,
        in_specs=(P("grp", ("row", "col"), None), P(), P(), P()),
        out_specs=P("grp", ("row", "col"), None),
        check_vma=False,
    )
```

profile of v0, /device:TPU:0, one launch (start us, length us, event | category | flops | bytes accessed | tf_op | source)
XLA Modules:
  0.0 68.8 jit_solution(5346477152302163925)
XLA Ops:
  0.0 1.4 %fusion.11 = f32[128]{0:T(128)S(1)} fusion(bf16[1,128,2048]{2,1,0:T(8,128)(2,1)} %param.4), kind=kLoop, calls=%fused_computation.22 | loop fusion | flops 786304 | bytes 524800 | tf_op jit(solution)/shard_map/reduce_sum | solution.py:53
  1.4 0.7 %convert_element_type.176 = f32[2048]{0:T(1024)S(1)} convert(bf16[2048]{0:T(1024)(128)(2,1)} %param.5) | non-fusion elementwise | flops 2048 | bytes 12288 | tf_op jit(solution)/shard_map/convert_element_type | solution.py:54
  2.1 2.3 %fusion.9 = bf16[512,128]{0,1:T(8,128)(2,1)S(1)} fusion(bf16[2048,512]{1,0:T(8,128)(2,1)} %param.6, bf16[1,128,2048]{2,1,0:T(8,128)(2,1)} %param.4, f32[2048]{0:T(1024)S(1)} %convert_element_type.176, f32[128]{0:T(128)S(1)} %add_rsqrt_fusion), kind=kOutput, calls=%fused_computation.20 | convolution fusion | flops 269549568 | bytes 2761216 | tf_op jit(solution)/shard_map/std,df->sft/dot_general | solution.py:55
  5.2 0.5 broadcast.304
  5.7 1.4 %reduce.2 = bf16[512,128]{1,0:T(8,128)(2,1)S(1)} reduce(bf16[512,1,128]{2,1,0:T(2,128)(2,1)S(1)} %bitcast.138, bf16[]{:T(256)} %broadcast.304), dimensions={1}, to_apply=%bitcast.133.reduce_sub_computation | reduce | bytes 262146
  7.1 0.7 reshape.272
  7.8 6.3 %all-to-all-start.1 = ((bf16[4,2,8192]{2,1,0:T(2,128)(2,1)}), bf16[4,2,8192]{2,1,0:T(2,128)(2,1)S(1)}, u32[]{:S(2)}, u32[]{:S(2)}) async-start(bf16[4,2,8192]{2,1,0:T(2,128)(2,1)} %reshape.272), calls=%async_computation.1 | async-start | bytes 262144 | tf_op jit(solution)/shard_map/all_to_all | solution.py:74
  14.8 1.4 %reduce.1 = bf16[512,128]{1,0:T(8,128)(2,1)S(1)} reduce(bf16[512,1,128]{2,1,0:T(2,128)(2,1)S(1)} %bitcast.139, bf16[]{:T(256)} %broadcast.304), dimensions={1}, to_apply=%bitcast.134.reduce_sub_computation | reduce | bytes 262146
  16.2 0.7 %reshape.270 = bf16[4,2,8192]{2,1,0:T(2,128)(2,1)} reshape(bf16[512,128]{1,0:T(8,128)(2,1)S(1)} %reduce.1) | data formatting | bytes 262144
  17.0 3.2 %all-to-all-done.1 = bf16[4,2,8192]{2,1,0:T(2,128)(2,1)S(1)} async-done(((bf16[4,2,8192]{2,1,0:T(2,128)(2,1)}), bf16[4,2,8192]{2,1,0:T(2,128)(2,1)S(1)}, u32[]{:S(2)}, u32[]{:S(2)}) %all-to-all-start.1) | async-done | bytes 131104 | tf_op jit(solution)/shard_map/all_to_all | solution.py:74
  20.2 3.3 %all-to-all-start = ((bf16[4,2,8192]{2,1,0:T(2,128)(2,1)}), bf16[4,2,8192]{2,1,0:T(2,128)(2,1)S(1)}, u32[]{:S(2)}, u32[]{:S(2)}) async-start(bf16[4,2,8192]{2,1,0:T(2,128)(2,1)} %reshape.270), calls=%async_computation | async-start | bytes 262144 | tf_op jit(solution)/shard_map/all_to_all | solution.py:71
  23.8 5.7 %all-to-all-done = bf16[4,2,8192]{2,1,0:T(2,128)(2,1)S(1)} async-done(((bf16[4,2,8192]{2,1,0:T(2,128)(2,1)}), bf16[4,2,8192]{2,1,0:T(2,128)(2,1)S(1)}, u32[]{:S(2)}, u32[]{:S(2)}) %all-to-all-start) | async-done | bytes 131104 | tf_op jit(solution)/shard_map/all_to_all | solution.py:71
  30.8 0.5 add_convert_fusion
  31.4 0.7 copy.31
  32.1 3.3 %all-to-all-start.3 = ((bf16[128,4,1,128]{3,0,2,1:T(8,128)(2,1)}), bf16[128,4,1,128]{3,0,2,1:T(8,128)(2,1)S(1)}, u32[]{:S(2)}, u32[]{:S(2)}) async-start(bf16[128,4,1,128]{3,0,2,1:T(8,128)(2,1)} %copy.31), calls=%async_computation.3 | async-start | bytes 262144 | tf_op jit(solution)/shard_map/all_to_all | solution.py:105
  35.4 0.7 copy.28
  36.1 3.9 %all-to-all-done.3 = bf16[128,4,1,128]{3,0,2,1:T(8,128)(2,1)S(1)} async-done(((bf16[128,4,1,128]{3,0,2,1:T(8,128)(2,1)}), bf16[128,4,1,128]{3,0,2,1:T(8,128)(2,1)S(1)}, u32[]{:S(2)}, u32[]{:S(2)}) %all-to-all-start.3) | async-done | bytes 131104 | tf_op jit(solution)/shard_map/all_to_all | solution.py:105
  40.0 3.3 %all-to-all-start.2 = ((bf16[128,4,1,128]{3,0,2,1:T(8,128)(2,1)}), bf16[128,4,1,128]{3,0,2,1:T(8,128)(2,1)S(1)}, u32[]{:S(2)}, u32[]{:S(2)}) async-start(bf16[128,4,1,128]{3,0,2,1:T(8,128)(2,1)} %copy.28), calls=%async_computation.2 | async-start | bytes 262144 | tf_op jit(solution)/shard_map/all_to_all | solution.py:102
  43.7 4.2 %all-to-all-done.2 = bf16[128,4,1,128]{3,0,2,1:T(8,128)(2,1)S(1)} async-done(((bf16[128,4,1,128]{3,0,2,1:T(8,128)(2,1)}), bf16[128,4,1,128]{3,0,2,1:T(8,128)(2,1)S(1)}, u32[]{:S(2)}, u32[]{:S(2)}) %all-to-all-start.2) | async-done | bytes 131104 | tf_op jit(solution)/shard_map/all_to_all | solution.py:102
  49.2 0.7 %fusion.19 = f32[128,4,4,32]{0,3,2,1:T(8,128)S(1)} fusion(f32[128,4,128,1]{2,1,0,3:T(4,128)S(1)} %get-tuple-element.6, s32[4,32]{1,0:T(4,128)S(1)} %multiply_add_fusion), kind=kOutput, calls=%fused_computation.29 | convolution fusion | flops 100892672 | bytes 524800 | tf_op jit(solution)/shard_map/rjt,qut->rjuq/dot_general | solution.py:26
  49.9 0.7 %fusion.10 = bf16[4,32,4,128]{3,1,0,2:T(8,128)(2,1)S(1)} fusion(f32[128,4,4,32]{0,3,2,1:T(8,128)S(1)} %fusion.19, f32[128,4,128,1]{2,1,0,3:T(4,128)S(1)} %get-tuple-element.5, s32[4,32]{1,0:T(4,128)S(1)} %multiply_add_fusion), kind=kOutput, calls=%fused_computation.21 | convolution fusion | flops 101089280 | bytes 655872 | tf_op jit(solution)/shard_map/rjt,qut->rjuq/dot_general | solution.py:26
  50.7 7.0 %all_to_all.78 = bf16[4,4,32,128,1]{3,2,0,4,1:T(8,128)(2,1)S(1)} all-to-all(bf16[4,4,32,128,1]{3,2,0,4,1:T(8,128)(2,1)S(1)} %copy.36), channel_id=1, replica_groups=mesh['grp'=2,'row'=4,'col'=4] {'col'}, dimensions={1} | all-to-all | bytes 262144 | tf_op jit(solution)/shard_map/all_to_all | solution.py:114
  58.3 8.6 %all_to_all.79 = bf16[4,32,1,4,128]{4,1,3,2,0:T(8,128)(2,1)S(1)} all-to-all(bf16[4,32,1,4,128]{4,1,3,2,0:T(8,128)(2,1)S(1)} %copy.39), channel_id=1, replica_groups=mesh['grp'=2,'row'=4,'col'=4] {'row'}, dimensions={0} | all-to-all | bytes 262144 | tf_op jit(solution)/shard_map/all_to_all | solution.py:116
  67.9 0.9 %reshape.260 = bf16[1,128,2048]{2,1,0:T(8,128)(2,1)} reshape(bf16[1,32,4,2048]{3,2,1,0:T(4,128)(2,1)S(1)} %copy.41) | data formatting | bytes 1048576 | tf_op jit(solution)/shard_map/reshape | solution.py:123
  (34 shorter events, 6.5 us)
Async XLA Ops:
  0.0 67.0 %copy-start = (bf16[512,2048]{1,0:T(8,128)(2,1)S(1)}, bf16[512,2048]{1,0:T(8,128)(2,1)}, u32[]{:S(2)}) copy-start(bf16[512,2048]{1,0:T(8,128)(2,1)} %param.7) | copy-start | bytes 6291460
  7.8 12.4 %all-to-all-start.1 = ((bf16[4,2,8192]{2,1,0:T(2,128)(2,1)}), bf16[4,2,8192]{2,1,0:T(2,128)(2,1)S(1)}, u32[]{:S(2)}, u32[]{:S(2)}) async-start(bf16[4,2,8192]{2,1,0:T(2,128)(2,1)} %reshape.272), calls=%async_computation.1 | async-start | bytes 262144 | tf_op jit(solution)/shard_map/all_to_all | solution.py:74
  20.2 9.2 %all-to-all-start = ((bf16[4,2,8192]{2,1,0:T(2,128)(2,1)}), bf16[4,2,8192]{2,1,0:T(2,128)(2,1)S(1)}, u32[]{:S(2)}, u32[]{:S(2)}) async-start(bf16[4,2,8192]{2,1,0:T(2,128)(2,1)} %reshape.270), calls=%async_computation | async-start | bytes 262144 | tf_op jit(solution)/shard_map/all_to_all | solution.py:71
  32.1 7.9 %all-to-all-start.3 = ((bf16[128,4,1,128]{3,0,2,1:T(8,128)(2,1)}), bf16[128,4,1,128]{3,0,2,1:T(8,128)(2,1)S(1)}, u32[]{:S(2)}, u32[]{:S(2)}) async-start(bf16[128,4,1,128]{3,0,2,1:T(8,128)(2,1)} %copy.31), calls=%async_computation.3 | async-start | bytes 262144 | tf_op jit(solution)/shard_map/all_to_all | solution.py:105
  40.0 7.9 %all-to-all-start.2 = ((bf16[128,4,1,128]{3,0,2,1:T(8,128)(2,1)}), bf16[128,4,1,128]{3,0,2,1:T(8,128)(2,1)S(1)}, u32[]{:S(2)}, u32[]{:S(2)}) async-start(bf16[128,4,1,128]{3,0,2,1:T(8,128)(2,1)} %copy.28), calls=%async_computation.2 | async-start | bytes 262144 | tf_op jit(solution)/shard_map/all_to_all | solution.py:102
where the time goes:
time: 69.5 us; the launch traced here: 68.8 us
  waiting for transfers between devices  16.9 us (24%)
  starting transfers between devices  16.3 us (23%)
  blocking collectives  15.5 us (22%)
  matrix products  8.52 us (12%)
  local copies, waits for them, and re-layouts  6.21 us (9%)
  other arithmetic  5.01 us (7%)
    all_to_all x1, blocking collectives, shards(): lax.all_to_all(returned.reshape(layout), 'row', split_axis=0, concat_axis...  8.56 us
    all_to_all x1, blocking collectives, shards(): lax.all_to_all(rounded, 'col', split_axis=1, concat_axis=4, tiled=True)  6.99 us
    all_to_all x1, starting transfers between devices, shards(): lax.all_to_all(spec_imag.astype(jnp.bfloat16), 'row', split_axis=1, conca...  6.35 us
    all_to_all x1, waiting for transfers between devices, shards(): lax.all_to_all(spec_real.astype(jnp.bfloat16), 'row', split_axis=1, conca...  5.68 us
    dot_general x10, matrix products, apply(): return jnp.einsum(pattern, table, data, precision=HIGHEST)  4.86 us
    all_to_all x1, waiting for transfers between devices, shards(): lax.all_to_all(sending[0].astype(jnp.bfloat16), 'col', split_axis=1, conc...  4.16 us
    all_to_all x1, waiting for transfers between devices, shards(): lax.all_to_all(sending[1].astype(jnp.bfloat16), 'col', split_axis=1, conc...  3.86 us
    all_to_all x1, starting transfers between devices, shards(): lax.all_to_all(spec_real.astype(jnp.bfloat16), 'row', split_axis=1, conca...  3.33 us
  transfers between devices with their start and end apart: 4, of which 4 were waited for; matrix products, arithmetic and copies ran while one was open for 6% of the time, Pallas kernels for 0%

commit v1 on v0

--- a/solution.py
+++ b/solution.py
@@ -1,8 +1,12 @@
+import functools
 import math
 
 import jax
 import jax.numpy as jnp
+import numpy as np
 from jax import lax
+from jax.experimental import pallas as pl
+from jax.experimental.pallas import tpu as pltpu
 from jax.sharding import PartitionSpec as P
 
 GROUP_CH = 128
@@ -38,7 +42,7 @@
     )
 
 
-def shards(tokens, norm_gain, w_in, w_out):
+def factored_shards(tokens, norm_gain, w_in, w_out):
     seq_count, tok_count, width = tokens.shape
     feat_count = w_in.shape[1]
     row_count = lax.axis_size("row")
@@ -123,6 +127,347 @@
     return mixed.reshape(seq_count, fine_count * row_count, width)
 
 
+LANES = 128
+SUBLANES = 8
+MESH = pl.DeviceIdType.MESH
+NT = (((1,), (1,)), ((), ()))
+
+
+def fused_fits(peers, tok_count, feat_count):
+    if feat_count % peers or tok_count % peers or GROUP_CH != LANES:
+        return False
+    slots = feat_count // peers
+    return (
+        tok_count == LANES
+        and slots % (4 * SUBLANES) == 0
+        and LANES % slots == 0
+        and peers % (LANES // slots) == 0
+        and feat_count % GROUP_CH == 0
+        and (tok_count // peers) % SUBLANES == 0
+    )
+
+
+def host_tables(peers, tok_count, feat_count):
+    length = peers * tok_count
+    slots = feat_count // peers
+    half = slots // 2
+    per_lane = LANES // slots
+    stacks = peers // per_lane
+    fine = tok_count // peers
+    members = GROUP_CH // slots
+    chan = np.zeros((GROUP_CH, GROUP_CH))
+    chan_at = np.zeros((GROUP_CH,), np.int64)
+    q = np.arange(GROUP_CH)
+    for m in range(GROUP_CH // 2):
+        row = m // half * slots + m % half
+        chan[row] = np.cos(2 * np.pi * (q * m % GROUP_CH) / GROUP_CH)
+        chan_at[row] = m
+        if m:
+            chan[row + half] = -np.sin(2 * np.pi * (q * m % GROUP_CH) / GROUP_CH)
+            chan_at[row + half] = GROUP_CH - m
+        else:
+            chan[row + half] = np.cos(np.pi * q)
+            chan_at[row + half] = GROUP_CH // 2
+    t = np.arange(tok_count)
+    b = np.arange(tok_count)[:, None]
+    scale = 1.0 / math.sqrt(length * GROUP_CH)
+    mid = np.zeros((stacks, tok_count, per_lane, 2, tok_count))
+    for g in range(stacks):
+        for a in range(per_lane):
+            k = peers * b + g * per_lane + a
+            angle = 2 * np.pi * (t * k % length) / length
+            mid[g, :, a, 0] = np.cos(angle) * scale
+            mid[g, :, a, 1] = np.sin(angle) * scale
+    mid = mid.reshape(stacks, tok_count, per_lane * 2 * tok_count)
+    pick = np.zeros((members, per_lane, slots, per_lane, GROUP_CH))
+    for dd in range(members):
+        for a in range(per_lane):
+            for c in range(slots):
+                pick[dd, a, c, a, chan_at[dd * slots + c]] = 1
+    pick = pick.reshape(members * LANES, per_lane * GROUP_CH)
+    order = np.zeros((tok_count, tok_count))
+    for a in range(per_lane):
+        for g in range(stacks):
+            for f in range(fine):
+                order[f * peers + g * per_lane + a, (a * stacks + g) * fine + f] = 1
+    return [jnp.asarray(x, jnp.bfloat16) for x in (chan, mid, pick, order)]
+
+
+def short_transform(blocks):
+    n = len(blocks)
+    even = [blocks[0]] + [blocks[s] + blocks[n - s] for s in range(1, n // 2)] + [blocks[n // 2]]
+    odd = [None] + [blocks[s] - blocks[n - s] for s in range(1, n // 2)]
+
+    def combine(terms):
+        groups = {}
+        for coef, term in terms:
+            if abs(coef) < 1e-9:
+                continue
+            size = round(abs(coef), 9)
+            signed = groups.get(size)
+            if signed is None:
+                groups[size] = term if coef > 0 else -term
+            else:
+                groups[size] = signed + term if coef > 0 else signed - term
+        total = None
+        for size, value in groups.items():
+            value = value if size == 1.0 else value * size
+            total = value if total is None else total + value
+        return total
+
+    out = []
+    for a in range(n // 2 + 1):
+        cos_part = combine(
+            [(math.cos(TWO_PI * (s * a % n) / n), even[s]) for s in range(n // 2 + 1)]
+        )
+        sin_part = combine([(math.sin(TWO_PI * (s * a % n) / n), odd[s]) for s in range(1, n // 2)])
+        if sin_part is None:
+            sin_part = jnp.zeros_like(cos_part)
+        out.append((cos_part, sin_part))
+    for a in range(n // 2 + 1, n):
+        out.append((out[n - a][0], -out[n - a][1]))
+    return out
+
+
+def fused_kernel(
+    shape,
+    tokens_hbm,
+    gain_hbm,
+    w_in_hbm,
+    w_out_hbm,
+    chan_hbm,
+    mid_hbm,
+    pick_hbm,
+    order_hbm,
+    out_ref,
+    tokens,
+    gain,
+    w_in,
+    w_out,
+    chan,
+    mid,
+    pick,
+    order,
+    first_out,
+    first_in,
+    blocks,
+    second_out,
+    second_in,
+    load_sem,
+    send_a,
+    recv_a,
+    send_b,
+    recv_b,
+):
+    row_count, col_count = shape
+    peers = row_count * col_count
+    tok_count, width = tokens.shape
+    feat_count = w_in.shape[1]
+    slots = feat_count // peers
+    half = slots // 2
+    per_lane = LANES // slots
+    stacks = peers // per_lane
+    fine = tok_count // peers
+    members = GROUP_CH // slots
+    groups = feat_count // GROUP_CH
+    me = lax.axis_index("row") * col_count + lax.axis_index("col")
+
+    def peer(step):
+        return lax.rem(me + step, peers)
+
+    def device(index):
+        return {"row": index // col_count, "col": lax.rem(index, col_count)}
+
+    chunks = 4
+    depth = width // chunks
+    loads = [
+        pltpu.make_async_copy(tokens_hbm, tokens, load_sem.at[0]),
+        pltpu.make_async_copy(gain_hbm, gain, load_sem.at[1]),
+    ]
+    for i in range(chunks):
+        part = pl.ds(i * depth, depth)
+        loads.append(pltpu.make_async_copy(w_in_hbm.at[part], w_in.at[part], load_sem.at[2 + i]))
+    rest = [(chan_hbm, chan), (mid_hbm, mid), (w_out_hbm, w_out), (pick_hbm, pick), (order_hbm, order)]
+    for i, (src, dst) in enumerate(rest):
+        loads.append(pltpu.make_async_copy(src, dst, load_sem.at[2 + chunks + i]))
+    for load in loads:
+        load.start()
+
+    barrier = pltpu.get_barrier_semaphore()
+    for step in range(1, peers):
+        pl.semaphore_signal(barrier, inc=1, device_id=device(peer(step)), device_id_type=MESH)
+
+    loads[0].wait()
+    loads[1].wait()
+    widened = tokens[...].astype(jnp.float32)
+    factor = lax.rsqrt(jnp.mean(widened * widened, -1, keepdims=True) + NORM_EPS)
+    normed = (widened * factor * gain[...].astype(jnp.float32)).astype(jnp.bfloat16)
+    mixin = None
+    for i in range(chunks):
+        loads[2 + i].wait()
+        term = jnp.dot(
+            normed[:, i * depth : (i + 1) * depth],
+            w_in[i * depth : (i + 1) * depth, :],
+            preferred_element_type=jnp.float32,
+        )
+        mixin = term if mixin is None else mixin + term
+    mixin = mixin.astype(jnp.bfloat16)
+    loads[2 + chunks].wait()
+    for g in range(groups):
+        spec = lax.dot_general(
+            chan[...],
+            mixin[:, g * GROUP_CH : (g + 1) * GROUP_CH],
+            NT,
+            preferred_element_type=jnp.float32,
+        ).astype(jnp.bfloat16)
+        for dd in range(members):
+            first_out[g * members + dd] = spec[dd * slots : (dd + 1) * slots]
+    pl.semaphore_wait(barrier, peers - 1)
+    copies = []
+    for step in range(1, peers):
+        target = peer(step)
+        copy = pltpu.make_async_remote_copy(
+            src_ref=first_out.at[target],
+            dst_ref=first_in.at[me],
+            send_sem=send_a.at[step],
+            recv_sem=recv_a.at[step],
+            device_id=device(target),
+            device_id_type=MESH,
+        )
+        copy.start()
+        copies.append(copy)
+    first_in[me] = first_out[me]
+    blocks[...] = jnp.zeros_like(blocks)
+    for load in loads[3 + chunks :]:
+        load.wait()
+    for copy in copies:
+        copy.wait_recv()
+
+    arrived = [first_in[s].astype(jnp.float32) for s in range(peers)]
+    place = lax.broadcasted_iota(jnp.int32, (half, tok_count), 0) + me * half
+    paired = lax.rem(place, GROUP_CH // 2) != 0
+    spectra = short_transform(arrived)
+    for a, (cos_part, sin_part) in enumerate(spectra):
+        a_cos, b_cos = cos_part[:half], cos_part[half:]
+        a_sin, b_sin = sin_part[:half], sin_part[half:]
+        top_cos = jnp.where(paired, a_cos + b_sin, a_cos)
+        top_sin = jnp.where(paired, b_cos - a_sin, -a_sin)
+        low_cos = jnp.where(paired, a_cos - b_sin, b_cos)
+        low_sin = jnp.where(paired, -a_sin - b_cos, -b_sin)
+        at = a % per_lane
+        left = at * 2 * tok_count
+        blocks[a // per_lane, at * slots : at * slots + half, left : left + tok_count] = (
+            top_cos.astype(jnp.bfloat16)
+        )
+        blocks[
+            a // per_lane, at * slots : at * slots + half, left + tok_count : left + 2 * tok_count
+        ] = top_sin.astype(jnp.bfloat16)
+        blocks[a // per_lane, at * slots + half : (at + 1) * slots, left : left + tok_count] = (
+            low_cos.astype(jnp.bfloat16)
+        )
+        blocks[
+            a // per_lane,
+            at * slots + half : (at + 1) * slots,
+            left + tok_count : left + 2 * tok_count,
+        ] = low_sin.astype(jnp.bfloat16)
+    found = []
+    for g in range(stacks):
+        value = lax.dot_general(mid[g], blocks[g], NT, preferred_element_type=jnp.float32)
+        found.append(value.reshape(peers, fine, LANES))
+    second_out[...] = jnp.concatenate(found, axis=1).astype(jnp.bfloat16)
+
+    def landing(index):
+        lanes = pl.ds(pl.multiple_of(lax.rem(index, members) * LANES, LANES), LANES)
+        return second_in.at[index // members, :, lanes]
+
+    returns = []
+    for step in range(1, peers):
+        target = peer(step)
+        copy = pltpu.make_async_remote_copy(
+            src_ref=second_out.at[target],
+            dst_ref=landing(me),
+            send_sem=send_b.at[step],
+            recv_sem=recv_b.at[step],
+            device_id=device(target),
+            device_id_type=MESH,
+        )
+        copy.start()
+        returns.append(copy)
+    landing(me)[...] = second_out[me]
+    for copy in copies:
+        copy.wait_send()
+    for copy in returns:
+        copy.wait_recv()
+    flat = second_in[...].reshape(groups * stacks * fine, members * LANES)
+    picked = jnp.dot(flat, pick[...], preferred_element_type=jnp.float32).astype(jnp.bfloat16)
+    rows = stacks * fine
+    gathered = jnp.concatenate(
+        [
+            jnp.concatenate(
+                [
+                    picked[g * rows : (g + 1) * rows, a * GROUP_CH : (a + 1) * GROUP_CH]
+                    for g in range(groups)
+                ],
+                axis=1,
+            )
+            for a in range(per_lane)
+        ],
+        axis=0,
+    )
+    spectrum = jnp.dot(order[...], gathered, preferred_element_type=jnp.float32).astype(
+        jnp.bfloat16
+    )
+    out_ref[...] = jnp.dot(spectrum, w_out[...], preferred_element_type=jnp.float32).astype(
+        out_ref.dtype
+    )
+    for copy in returns:
+        copy.wait_send()
+
+
+def fused_shards(tokens, norm_gain, w_in, w_out):
+    seq_count, tok_count, width = tokens.shape
+    feat_count = w_in.shape[1]
+    shape = (lax.axis_size("row"), lax.axis_size("col"))
+    peers = shape[0] * shape[1]
+    slots = feat_count // peers
+    per_lane = LANES // slots
+    stacks = peers // per_lane
+    fine = tok_count // peers
+    members = GROUP_CH // slots
+    tables = host_tables(peers, tok_count, feat_count)
+    operands = [tokens.reshape(tok_count, width), norm_gain.reshape(1, width), w_in, w_out, *tables]
+    held = [pltpu.VMEM(x.shape, x.dtype) for x in operands]
+    mixed = pl.pallas_call(
+        functools.partial(fused_kernel, shape),
+        out_shape=jax.ShapeDtypeStruct((tok_count, width), jnp.bfloat16),
+        in_specs=[pl.BlockSpec(memory_space=pl.ANY)] * len(operands),
+        out_specs=pl.BlockSpec(memory_space=pltpu.VMEM),
+        scratch_shapes=held
+        + [
+            pltpu.VMEM((peers, slots, tok_count), jnp.bfloat16),
+            pltpu.VMEM((peers, slots, tok_count), jnp.bfloat16),
+            pltpu.VMEM((stacks, LANES, per_lane * 2 * tok_count), jnp.bfloat16),
+            pltpu.VMEM((peers, stacks * fine, LANES), jnp.bfloat16),
+            pltpu.VMEM((peers // members, stacks * fine, members * LANES), jnp.bfloat16),
+            pltpu.SemaphoreType.DMA((16,)),
+            pltpu.SemaphoreType.DMA((peers,)),
+            pltpu.SemaphoreType.DMA((peers,)),
+            pltpu.SemaphoreType.DMA((peers,)),
+            pltpu.SemaphoreType.DMA((peers,)),
+        ],
+        compiler_params=pltpu.CompilerParams(collective_id=0, has_side_effects=True),
+    )(*operands)
+    return mixed.reshape(seq_count, tok_count, width)
+
+
+def shards(tokens, norm_gain, w_in, w_out):
+    peers = lax.axis_size("row") * lax.axis_size("col")
+    seq_count, tok_count, _ = tokens.shape
+    if seq_count == 1 and fused_fits(peers, tok_count, w_in.shape[1]):
+        return fused_shards(tokens, norm_gain, w_in, w_out)
+    return factored_shards(tokens, norm_gain, w_in, w_out)
+
+
 def solution(mesh):
     return jax.shard_map(
         shards,

time: 69.5 us -> 21.7 us (0.31)
  Pallas kernels: 0 us -> 18.4 us
  waiting for transfers between devices: 16.9 us -> 0 us
  starting transfers between devices: 16.3 us -> 0 us
  blocking collectives: 15.5 us -> 0 us
  matrix products: 8.52 us -> 0 us
  other arithmetic: 5.01 us -> 0 us
  local copies, waits for them, and re-layouts: 6.21 us -> 3.17 us
    pallas_call x0 -> x1, Pallas kernels: none -> 18.4 us  [fused_shards(): pl.pallas_call(functools.partial(fused_kernel, shape), out_shape=jax.Shap...]
    all_to_all x4 -> x0, waiting for transfers between devices: 16.9 us -> none  [the longest x1 5.68 us: shards(): lax.all_to_all(spec_real.astype(jnp.bfloat16), 'row', split_axis=1, conca...]
    all_to_all x4 -> x0, starting transfers between devices: 16.3 us -> none  [the longest x1 6.35 us: shards(): lax.all_to_all(spec_imag.astype(jnp.bfloat16), 'row', split_axis=1, conca...]
    all_to_all x2 -> x0, blocking collectives: 15.5 us -> none  [the longest x1 8.56 us: shards(): lax.all_to_all(returned.reshape(layout), 'row', split_axis=0, concat_axis...]
    dot_general x14 -> x0, matrix products: 8.52 us -> none  [the longest x10 4.86 us: apply(): return jnp.einsum(pattern, table, data, precision=HIGHEST)]
    unnamed x2 -> x0, other arithmetic: 2.82 us -> none
    convert_element_type x9 -> x0, local copies, waits for them, and re-layouts: 2.32 us -> none  [the longest x2 0.69 us: shards(): sending[1].astype(jnp.bfloat16)]
    reduce_sum x1 -> x0, other arithmetic: 1.38 us -> none  [shards(): jnp.mean(widened * widened, -1, keepdims=True) + NORM_EPS]
  transfers between devices with their start and end apart: 4 -> 0, of which waited for: 4 -> 0; matrix products, arithmetic and copies ran while one was open for 6% -> 0% of each run, Pallas kernels for 0% -> 0%
where the time goes in v1:
time: 21.7 us; the launch traced here: 21.5 us
  Pallas kernels  18.4 us (85%)
  local copies, waits for them, and re-layouts  3.17 us (15%)
    pallas_call x1, Pallas kernels, fused_shards(): pl.pallas_call(functools.partial(fused_kernel, shape), out_shape=jax.Shap...  18.4 us
    unnamed x1, local copies, waits for them, and re-layouts  1.88 us
    reshape x1, local copies, waits for them, and re-layouts, fused_shards(): norm_gain.reshape(1, width)  1.29 us

profile of v1, /device:TPU:0, one launch (start us, length us, event | category | flops | bytes accessed | tf_op | source)
XLA Modules:
  0.0 21.5 jit_solution(1166530497055768242)
XLA Ops:
  0.0 1.3 %reshape.10.gain_hbm = bf16[1,2048]{1,0:T(2,128)(2,1)} reshape(bf16[2048]{0:T(1024)(128)(2,1)} %param.9) | data formatting | bytes 8192 | tf_op jit(solution)/shard_map/reshape | solution.py:438
  1.3 18.4 %shard_map.82 = bf16[128,2048]{1,0:T(8,128)(2,1)} custom-call(bf16[128,2048]{1,0:T(8,128)(2,1)} %bitcast.3, bf16[1,2048]{1,0:T(2,128)(2,1)} %reshape.10.gain_hbm, bf16[2048,512]{1,0:T(8,128)(2,1)} %w_in_hbm.1, bf16[512,2048]{1,0:T(8,128)(2,1)} %w_out_hbm.1, bf16[128,128]{1,0:T(8,128)(2,1)} %constant.8.clone.chan_hbm, ...), custom_call_target="tpu_custom_call" | custom-call | tf_op jit(solution)/shard_map/pallas_call | solution.py:440
  19.7 1.9 %copy.10 = bf16[1,128,2048]{2,1,0:T(8,128)(2,1)} copy(bf16[1,128,2048]{2,1,0:T(8,128)(2,1)} %bitcast.2) | data formatting | bytes 1048576

commit v2 on v1

--- a/solution.py
+++ b/solution.py
@@ -185,12 +185,7 @@
             for c in range(slots):
                 pick[dd, a, c, a, chan_at[dd * slots + c]] = 1
     pick = pick.reshape(members * LANES, per_lane * GROUP_CH)
-    order = np.zeros((tok_count, tok_count))
-    for a in range(per_lane):
-        for g in range(stacks):
-            for f in range(fine):
-                order[f * peers + g * per_lane + a, (a * stacks + g) * fine + f] = 1
-    return [jnp.asarray(x, jnp.bfloat16) for x in (chan, mid, pick, order)]
+    return [jnp.asarray(x, jnp.bfloat16) for x in (chan, mid, pick)]
 
 
 def short_transform(blocks):
@@ -234,20 +229,17 @@
     tokens_hbm,
     gain_hbm,
     w_in_hbm,
-    w_out_hbm,
     chan_hbm,
     mid_hbm,
     pick_hbm,
-    order_hbm,
     out_ref,
     tokens,
     gain,
     w_in,
-    w_out,
     chan,
     mid,
     pick,
-    order,
+    natural,
     first_out,
     first_in,
     blocks,
@@ -287,10 +279,10 @@
     for i in range(chunks):
         part = pl.ds(i * depth, depth)
         loads.append(pltpu.make_async_copy(w_in_hbm.at[part], w_in.at[part], load_sem.at[2 + i]))
-    rest = [(chan_hbm, chan), (mid_hbm, mid), (w_out_hbm, w_out), (pick_hbm, pick), (order_hbm, order)]
+    rest = [(chan_hbm, chan), (mid_hbm, mid), (pick_hbm, pick)]
     for i, (src, dst) in enumerate(rest):
         loads.append(pltpu.make_async_copy(src, dst, load_sem.at[2 + chunks + i]))
-    for load in loads:
+    for load in loads[: 3 + chunks]:
         load.start()
 
     barrier = pltpu.get_barrier_semaphore()
@@ -301,7 +293,7 @@
     loads[1].wait()
     widened = tokens[...].astype(jnp.float32)
     factor = lax.rsqrt(jnp.mean(widened * widened, -1, keepdims=True) + NORM_EPS)
-    normed = (widened * factor * gain[...].astype(jnp.float32)).astype(jnp.bfloat16)
+    normed = (widened * factor * gain[...].astype(jnp.float32).reshape(1, width)).astype(jnp.bfloat16)
     mixin = None
     for i in range(chunks):
         loads[2 + i].wait()
@@ -312,6 +304,8 @@
         )
         mixin = term if mixin is None else mixin + term
     mixin = mixin.astype(jnp.bfloat16)
+    for load in loads[3 + chunks :]:
+        load.start()
     loads[2 + chunks].wait()
     for g in range(groups):
         spec = lax.dot_general(
@@ -399,29 +393,33 @@
     for copy in returns:
         copy.wait_recv()
     flat = second_in[...].reshape(groups * stacks * fine, members * LANES)
-    picked = jnp.dot(flat, pick[...], preferred_element_type=jnp.float32).astype(jnp.bfloat16)
-    rows = stacks * fine
-    gathered = jnp.concatenate(
-        [
-            jnp.concatenate(
-                [
-                    picked[g * rows : (g + 1) * rows, a * GROUP_CH : (a + 1) * GROUP_CH]
-                    for g in range(groups)
-                ],
-                axis=1,
-            )
-            for a in range(per_lane)
-        ],
-        axis=0,
-    )
-    spectrum = jnp.dot(order[...], gathered, preferred_element_type=jnp.float32).astype(
-        jnp.bfloat16
-    )
-    out_ref[...] = jnp.dot(spectrum, w_out[...], preferred_element_type=jnp.float32).astype(
-        out_ref.dtype
-    )
+    picked = jnp.dot(flat, pick[...], preferred_element_type=jnp.float32)
+    for group in range(groups):
+        for g in range(stacks):
+            top = (group * stacks + g) * fine
+            for a in range(per_lane):
+                natural[group, pl.ds(g * per_lane + a, fine, stride=peers), :] = picked[top : top + fine, a * GROUP_CH : (a + 1) * GROUP_CH]
+        out_ref[:, group * GROUP_CH : (group + 1) * GROUP_CH] = natural[group].astype(
+            out_ref.dtype
+        )
     for copy in returns:
         copy.wait_send()
+
+
+def project_kernel(chunks, spectrum, w_out, out_hbm, staged, sems):
+    size = w_out.shape[1] // chunks
+    copies = []
+    for i in range(chunks):
+        lanes = slice(i * size, (i + 1) * size)
+        staged[:, lanes] = jnp.dot(
+            spectrum[...], w_out[:, lanes], preferred_element_type=jnp.float32
+        ).astype(staged.dtype)
+        span = pl.ds(i * size, size)
+        copy = pltpu.make_async_copy(staged.at[:, span], out_hbm.at[:, span], sems.at[i])
+        copy.start()
+        copies.append(copy)
+    for copy in copies:
+        copy.wait()
 
 
 def fused_shards(tokens, norm_gain, w_in, w_out):
@@ -435,15 +433,16 @@
     fine = tok_count // peers
     members = GROUP_CH // slots
     tables = host_tables(peers, tok_count, feat_count)
-    operands = [tokens.reshape(tok_count, width), norm_gain.reshape(1, width), w_in, w_out, *tables]
+    operands = [tokens.reshape(tok_count, width), norm_gain, w_in, *tables]
     held = [pltpu.VMEM(x.shape, x.dtype) for x in operands]
-    mixed = pl.pallas_call(
+    spectrum = pl.pallas_call(
         functools.partial(fused_kernel, shape),
-        out_shape=jax.ShapeDtypeStruct((tok_count, width), jnp.bfloat16),
-        in_specs=[pl.BlockSpec(memory_space=pl.ANY)] * len(operands),
+        out_shape=pltpu.VMEM((tok_count, feat_count), jnp.bfloat16),
+        in_specs=[pl.BlockSpec(memory_space=pltpu.HBM)] * len(operands),
         out_specs=pl.BlockSpec(memory_space=pltpu.VMEM),
         scratch_shapes=held
         + [
+            pltpu.VMEM((feat_count // GROUP_CH, tok_count, GROUP_CH), jnp.float32),
             pltpu.VMEM((peers, slots, tok_count), jnp.bfloat16),
             pltpu.VMEM((peers, slots, tok_count), jnp.bfloat16),
             pltpu.VMEM((stacks, LANES, per_lane * 2 * tok_count), jnp.bfloat16),
@@ -455,8 +454,22 @@
             pltpu.SemaphoreType.DMA((peers,)),
             pltpu.SemaphoreType.DMA((peers,)),
         ],
-        compiler_params=pltpu.CompilerParams(collective_id=0, has_side_effects=True),
+        compiler_params=pltpu.CompilerParams(
+            collective_id=0, has_side_effects=True, vmem_limit_bytes=64_600_000
+        ),
     )(*operands)
+    chunks = max(1, width // 512)
+    mixed = pl.pallas_call(
+        functools.partial(project_kernel, chunks),
+        out_shape=jax.ShapeDtypeStruct((tok_count, width), jnp.bfloat16),
+        in_specs=[pl.BlockSpec(memory_space=pltpu.VMEM)] * 2,
+        out_specs=pl.BlockSpec(memory_space=pltpu.HBM),
+        scratch_shapes=[
+            pltpu.VMEM((tok_count, width), jnp.bfloat16),
+            pltpu.SemaphoreType.DMA((chunks,)),
+        ],
+        compiler_params=pltpu.CompilerParams(vmem_limit_bytes=8 * 1024 * 1024),
+    )(spectrum, w_out)
     return mixed.reshape(seq_count, tok_count, width)
 
 

time: 21.7 us -> 18.4 us (0.85)
  local copies, waits for them, and re-layouts: 3.17 us -> 0.01 us
    unnamed x1 -> x2, local copies, waits for them, and re-layouts: 1.88 us -> 0.01 us
    reshape x1 -> x0, local copies, waits for them, and re-layouts: 1.29 us -> none  [fused_shards(): norm_gain.reshape(1, width)]
    pallas_call x1 -> x2, Pallas kernels: 18.4 us -> 18.3 us  [the longest x1 17.1 us: fused_shards(): pl.pallas_call(functools.partial(fused_kernel, shape), out_shape=pltpu.VM...]
where the time goes in v2:
time: 18.4 us; the launch traced here: 18.3 us
  Pallas kernels  18.3 us (99%)
    pallas_call x1, Pallas kernels, fused_shards(): pl.pallas_call(functools.partial(fused_kernel, shape), out_shape=pltpu.VM...  17.1 us
    pallas_call x1, Pallas kernels, fused_shards(): pl.pallas_call(functools.partial(project_kernel, chunks), out_shape=jax.S...  1.15 us

profile of v2, /device:TPU:0, one launch (start us, length us, event | category | flops | bytes accessed | tf_op | source)
XLA Modules:
  0.0 18.3 jit_solution(2030634494784613587)
XLA Ops:
  0.0 0.0 copy-start
  0.0 17.1 %shard_map.73.spectrum = bf16[128,512]{1,0:T(8,128)(2,1)S(1)} custom-call(bf16[128,2048]{1,0:T(8,128)(2,1)} %bitcast.2, bf16[2048]{0:T(1024)(128)(2,1)} %gain_hbm.1, bf16[2048,512]{1,0:T(8,128)(2,1)} %w_in_hbm.1, bf16[128,128]{1,0:T(8,128)(2,1)} %constant.6.clone.chan_hbm, bf16[4,128,1024]{2,1,0:T(8,128)(2,1)} %constant.7.clone.mid_hbm, ...), custom_call_target="tpu_custom_call" | custom-call | tf_op jit(solution)/shard_map/pallas_call | solution.py:438
  17.1 0.0 copy-done
  17.2 1.1 %shard_map.74 = bf16[128,2048]{1,0:T(8,128)(2,1)} custom-call(bf16[128,512]{1,0:T(8,128)(2,1)S(1)} %shard_map.73.spectrum, bf16[512,2048]{1,0:T(8,128)(2,1)S(1)} %copy-done), custom_call_target="tpu_custom_call" | custom-call | tf_op jit(solution)/shard_map/pallas_call | solution.py:462
Async XLA Ops:
  0.0 17.2 %copy-start = (bf16[512,2048]{1,0:T(8,128)(2,1)S(1)}, bf16[512,2048]{1,0:T(8,128)(2,1)}, u32[]{:S(2)}) copy-start(bf16[512,2048]{1,0:T(8,128)(2,1)} %w_out.1) | copy-start | bytes 6291460

commit v3 on v2

--- a/solution.py
+++ b/solution.py
@@ -270,6 +270,19 @@
     def device(index):
         return {"row": index // col_count, "col": lax.rem(index, col_count)}
 
+    row, col = lax.axis_index("row"), lax.axis_index("col")
+    far_first = []
+    for i in range(row_count - 1):
+        down = row_count - 1 - i
+        down = down - jnp.where(down <= row, 1, 0)
+        up = i + jnp.where(i >= row, 1, 0)
+        target_row = jnp.where(row * 2 < row_count, down, up)
+        far_first += [
+            target_row * col_count + lax.rem(col + shift, col_count)
+            for shift in [*range(1, col_count), 0]
+        ]
+    far_first += [row * col_count + lax.rem(col + shift, col_count) for shift in range(1, col_count)]
+
     chunks = 4
     depth = width // chunks
     loads = [
@@ -318,13 +331,12 @@
             first_out[g * members + dd] = spec[dd * slots : (dd + 1) * slots]
     pl.semaphore_wait(barrier, peers - 1)
     copies = []
-    for step in range(1, peers):
-        target = peer(step)
+    for step, target in enumerate(far_first):
         copy = pltpu.make_async_remote_copy(
             src_ref=first_out.at[target],
             dst_ref=first_in.at[me],
             send_sem=send_a.at[step],
-            recv_sem=recv_a.at[step],
+            recv_sem=recv_a.at[me],
             device_id=device(target),
             device_id_type=MESH,
         )
@@ -334,8 +346,9 @@
     blocks[...] = jnp.zeros_like(blocks)
     for load in loads[3 + chunks :]:
         load.wait()
-    for copy in copies:
-        copy.wait_recv()
+    for step in range(1, peers):
+        source = peer(step)
+        pltpu.make_async_copy(first_in.at[source], first_in.at[source], recv_a.at[source]).wait()
 
     arrived = [first_in[s].astype(jnp.float32) for s in range(peers)]
     place = lax.broadcasted_iota(jnp.int32, (half, tok_count), 0) + me * half
@@ -375,13 +388,12 @@
         return second_in.at[index // members, :, lanes]
 
     returns = []
-    for step in range(1, peers):
-        target = peer(step)
+    for step, target in enumerate(far_first):
         copy = pltpu.make_async_remote_copy(
             src_ref=second_out.at[target],
             dst_ref=landing(me),
             send_sem=send_b.at[step],
-            recv_sem=recv_b.at[step],
+            recv_sem=recv_b.at[me],
             device_id=device(target),
             device_id_type=MESH,
         )
@@ -390,8 +402,9 @@
     landing(me)[...] = second_out[me]
     for copy in copies:
         copy.wait_send()
-    for copy in returns:
-        copy.wait_recv()
+    for step in range(1, peers):
+        source = peer(step)
+        pltpu.make_async_copy(landing(source), landing(source), recv_b.at[source]).wait()
     flat = second_in[...].reshape(groups * stacks * fine, members * LANES)
     picked = jnp.dot(flat, pick[...], preferred_element_type=jnp.float32)
     for group in range(groups):

time: 18.4 us -> 18.4 us (level)
  no operation moved by 1% of the time
where the time goes in v3:
time: 18.4 us; the launch traced here: 18.2 us
  Pallas kernels  18.2 us (99%)
    pallas_call x1, Pallas kernels, fused_shards(): pl.pallas_call(functools.partial(fused_kernel, shape), out_shape=pltpu.VM...  17 us
    pallas_call x1, Pallas kernels, fused_shards(): pl.pallas_call(functools.partial(project_kernel, chunks), out_shape=jax.S...  1.15 us

profile of v3, /device:TPU:0, one launch (start us, length us, event | category | flops | bytes accessed | tf_op | source)
XLA Modules:
  0.0 18.2 jit_solution(2852789495797584162)
XLA Ops:
  0.0 0.0 copy-start
  0.0 17.0 %shard_map.73.spectrum = bf16[128,512]{1,0:T(8,128)(2,1)S(1)} custom-call(bf16[128,2048]{1,0:T(8,128)(2,1)} %bitcast.2, bf16[2048]{0:T(1024)(128)(2,1)} %gain_hbm.1, bf16[2048,512]{1,0:T(8,128)(2,1)} %w_in_hbm.1, bf16[128,128]{1,0:T(8,128)(2,1)} %constant.6.clone.chan_hbm, bf16[4,128,1024]{2,1,0:T(8,128)(2,1)} %constant.7.clone.mid_hbm, ...), custom_call_target="tpu_custom_call" | custom-call | tf_op jit(solution)/shard_map/pallas_call | solution.py:451
  17.1 0.0 copy-done
  17.1 1.1 %shard_map.74 = bf16[128,2048]{1,0:T(8,128)(2,1)} custom-call(bf16[128,512]{1,0:T(8,128)(2,1)S(1)} %shard_map.73.spectrum, bf16[512,2048]{1,0:T(8,128)(2,1)S(1)} %copy-done), custom_call_target="tpu_custom_call" | custom-call | tf_op jit(solution)/shard_map/pallas_call | solution.py:475
Async XLA Ops:
  0.0 17.1 %copy-start = (bf16[512,2048]{1,0:T(8,128)(2,1)S(1)}, bf16[512,2048]{1,0:T(8,128)(2,1)}, u32[]{:S(2)}) copy-start(bf16[512,2048]{1,0:T(8,128)(2,1)} %w_out.1) | copy-start | bytes 6291460
